TPU v7x, 32 devices: a whole 2x2x4 slice. The times are simulated.
32 devices in a mesh: rep: 4 (over z), fs: 4 (over y, x), tp: 2 (over core).
Axes of the slice: x: 2, y: 2, z: 4, core: 2. Of those that a mesh axis runs over, the one named last changes fastest.
Arguments:
- inputs: bfloat16 [512, 2048], P(('rep', 'fs', 'tp')), may hold values from -6 to 6
- cotangent: bfloat16 [512, 2048], P(('rep', 'fs', 'tp')), may hold values from -6 to 6
- norm_gain: float32 [2048], replicated, may hold values from 0.1 to 1.9
- gate_weight: bfloat16 [2048, 2816], P(None, ('fs', 'tp')), may hold values from -0.125 to 0.125
- up_weight: bfloat16 [2048, 2816], P(None, ('fs', 'tp')), may hold values from -0.125 to 0.125
- down_weight: bfloat16 [2816, 2048], P(('fs', 'tp')), may hold values from -0.109375 to 0.109375
Outputs:
- input_grad: bfloat16 [512, 2048], P(('rep', 'fs', 'tp'))
- gain_grad: float32 [2048], replicated
- down_grad: float32 [2816, 2048], P(('fs', 'tp'), 'rep')
All inputs are finite; a program needn't handle non-finite values.
Results may differ from a plain program's by a relative error of at most 0.0066.
Values may be sent and summed in bfloat16 or wider, within the bound.
A program may use at most 64 MiB of HBM per device.

v0:
```python
import jax
import jax.numpy as jnp
from jax import lax
from jax.sharding import PartitionSpec as P

EPS = 1e-06


def across_tokens(left, right):
    return lax.dot_general(
        left, right, (((0,), (0,)), ((), ())), preferred_element_type=jnp.float32
    )


def across_columns(left, right):
    return lax.dot_general(
        left, right, (((1,), (1,)), ((), ())), preferred_element_type=jnp.float32
    )


def per_device(inputs, cotangent, norm_gain, gate_weight, up_weight, down_weight):
    whole_x, whole_dy = (
        lax.all_gather(inputs, ("fs", "tp"), axis=0, tiled=True),
        lax.all_gather(cotangent, ("fs", "tp"), axis=0, tiled=True),
    )
    xf = whole_x.astype(jnp.float32)
    inv = lax.rsqrt(jnp.mean(xf * xf, axis=-1, keepdims=True) + EPS)
    normed = xf * inv
    hidden_in = (normed * norm_gain).astype(jnp.bfloat16)
    gate = jnp.dot(hidden_in, gate_weight, preferred_element_type=jnp.float32)
    up = jnp.dot(hidden_in, up_weight, preferred_element_type=jnp.float32)
    sig = jax.nn.sigmoid(gate)
    act = gate * sig
    hidden = (act * up).astype(jnp.bfloat16)
    d_hidden = 0.5 * across_columns(whole_dy, down_weight)
    d_gate = (d_hidden * up * sig * (1.0 + gate * (1.0 - sig))).astype(jnp.bfloat16)
    d_up = (d_hidden * act).astype(jnp.bfloat16)
    own_rows = inputs.shape[0]
    d_in = lax.psum_scatter(
        across_columns(d_gate, gate_weight) + across_columns(d_up, up_weight),
        ("fs", "tp"),
        scatter_dimension=0,
        tiled=True,
    )
    offset = lax.axis_index(("fs", "tp")) * own_rows
    own_normed = lax.dynamic_slice_in_dim(normed, offset, own_rows, 0)
    own_inv = lax.dynamic_slice_in_dim(inv, offset, own_rows, 0)
    gain_grad = lax.psum(jnp.sum(d_in * own_normed, axis=0), ("rep", "fs", "tp"))
    scaled = d_in * norm_gain
    input_grad = (
        own_inv * (scaled - own_normed * jnp.mean(scaled * own_normed, axis=-1, keepdims=True))
    ).astype(jnp.bfloat16)
    input_grad, gain_grad = (input_grad, gain_grad)
    part_down = 0.5 * across_tokens(whole_dy, hidden)
    got_down = lax.all_to_all(
        part_down[None].astype(jnp.bfloat16), "rep", split_axis=1, concat_axis=0, tiled=True
    ).astype(jnp.float32)
    down_grad = jnp.sum(got_down, axis=0).T
    return (input_grad, gain_grad, down_grad)


def solution(mesh):
    return jax.shard_map(
        per_device,
        mesh=mesh,
        in_specs=(
            P(("rep", "fs", "tp"), None),
            P(("rep", "fs", "tp"), None),
            P(),
            P(None, ("fs", "tp")),
            P(None, ("fs", "tp")),
            P(("fs", "tp"), None),
        ),
        out_specs=(P(("rep", "fs", "tp"), None), P(), P(("fs", "tp"), "rep")),
        check_vma=False,
    )
```

profile of v0, /device:TPU:0, one launch (start us, length us, event | category | flops | bytes accessed | tf_op | source)
XLA Modules:
  0.0 166.7 jit_solution(2304956729085242355)
XLA Ops:
  7.2 11.8 %all_gather.6 = bf16[128,2048]{1,0:T(8,128)(2,1)S(1)} all-gather(bf16[16,2048]{1,0:T(8,128)(2,1)} %param.6), channel_id=1, replica_groups=mesh['rep'=4,'fs'=4,'tp'=2] {'fs','tp'}, dimensions={0}, use_global_device_ids=true | all-gather | bytes 589824 | tf_op jit(solution)/shard_map/all_gather | solution.py:23
  19.0 0.2 fusion.2
  19.2 1.4 fusion.3
  20.7 0.6 fusion.4
  21.3 0.3 copy-done.6
  21.6 9.5 %all_gather.7 = bf16[128,2048]{1,0:T(8,128)(2,1)S(1)} all-gather(bf16[16,2048]{1,0:T(8,128)(2,1)S(1)} %copy-done.6), channel_id=1, replica_groups=mesh['rep'=4,'fs'=4,'tp'=2] {'fs','tp'}, dimensions={0}, use_global_device_ids=true | all-gather | bytes 589824 | tf_op jit(solution)/shard_map/all_gather | solution.py:24
  31.1 0.8 copy-done.1
  31.9 0.5 convolution_multiply_fusion.1
  32.4 0.5 fusion.6
  33.0 1.5 convolution_add_fusion
  34.5 1.8 %fusion.1 = bf16[1,2048,352]{1,2,0:T(8,128)(2,1)S(1)} fusion(bf16[128,2048]{1,0:T(8,128)(2,1)} %copy-done.1, f32[128,352]{0,1:T(8,128)} %copy-done.5, f32[128,352]{0,1:T(8,128)} %copy-done.2), kind=kOutput, calls=%fused_computation.2 | convolution fusion | flops 186261504 | bytes 2326528 | tf_op jit(solution)/shard_map/dot_general | solution.py:10
  36.3 5.7 %copy.12 = bf16[1,2048,352]{2,0,1:T(2,128)(2,1)} copy(bf16[1,2048,352]{1,2,0:T(8,128)(2,1)S(1)} %fusion.1) | data formatting | bytes 2883584 | tf_op jit(solution)/shard_map/convert_element_type | solution.py:56
  42.0 0.5 broadcast.53
  42.5 34.4 %reduce = bf16[2048,352]{1,0:T(8,128)(2,1)S(1)} reduce(bf16[2048,1,352]{2,1,0:T(2,128)(2,1)} %bitcast.16, bf16[]{:T(256)} %broadcast.53), dimensions={1}, to_apply=%bitcast.7.reduce_sub_computation | reduce | bytes 2883586
  76.9 3.6 %reshape.41 = bf16[4,2,90112]{2,1,0:T(2,128)(2,1)} reshape(bf16[2048,352]{1,0:T(8,128)(2,1)S(1)} %reduce) | data formatting | bytes 2883584
  80.5 4.9 %all-to-all-start = ((bf16[4,2,90112]{2,1,0:T(2,128)(2,1)}), bf16[4,2,90112]{2,1,0:T(2,128)(2,1)S(1)}, u32[]{:S(2)}, u32[]{:S(2)}) async-start(bf16[4,2,90112]{2,1,0:T(2,128)(2,1)} %reshape.41), calls=%async_computation.1 | async-start | bytes 2883584 | tf_op jit(solution)/shard_map/all_to_all | solution.py:55
  85.4 1.1 convert_multiply_fusion
  86.5 1.1 multiply_reduce_fusion
  87.6 51.7 %psum.7 = f32[2048]{0:T(1024)} all-reduce(f32[2048]{0:T(1024)S(1)} %get-tuple-element.3), channel_id=1, replica_groups=mesh['rep'=4,'fs'=4,'tp'=2] {'rep','fs','tp'}, use_global_device_ids=true, to_apply=%region_4.0 | all-reduce | flops 2048 | bytes 16384 | tf_op jit(solution)/shard_map/psum | solution.py:48
  139.4 1.7 %multiply_convert_fusion.6 = bf16[16,2048]{1,0:T(8,128)(2,1)} fusion(f32[16,2048]{1,0:T(8,128)} %reduce-scatter.2.cloned.1.call-done, f32[128,2048]{1,0:T(8,128)} %convert_multiply_fusion, s32[]{:T(128)S(6)} %select_n.4, f32[16]{0:T(128)S(1)} %broadcast_multiply_fusion, f32[2048]{0:T(1024)S(1)} %copy-done.7, f32[16]{0:T(128)S(1)} %dynamic-slice.3), kind=kLoop, calls=%fused_computation.17 | loop fusion | flops 163840 | bytes 336004 | tf_op jit(solution)/shard_map/convert_element_type | solution.py:52
  141.1 4.0 %reshape.42 = bf16[2048,1,352]{2,1,0:T(2,128)(2,1)} reshape(bf16[4,2,90112]{2,1,0:T(2,128)(2,1)S(1)} %all-to-all-done) | data formatting | bytes 2883584
  145.0 7.0 %copy.13 = bf16[1,2048,352]{1,2,0:T(8,128)(2,1)S(1)} copy(bf16[1,2048,352]{2,0,1:T(2,128)(2,1)} %bitcast.17) | data formatting | bytes 2883584 | tf_op jit(solution)/shard_map/all_to_all | solution.py:55
  152.0 3.4 %reshape.40 = f32[4,512,352]{1,0,2:T(4,128)} reshape(bf16[1,2048,352]{1,2,0:T(8,128)(2,1)S(1)} %copy.13) | data formatting | bytes 4325376 | tf_op jit(solution)/shard_map/convert_element_type | solution.py:57
  155.5 4.4 %reduce_sum.39 = f32[512,352]{0,1:T(8,128)} reduce(f32[4,512,352]{1,0,2:T(4,128)} %reshape.40, f32[]{:T(128)} %constant.11.clone.1), dimensions={0}, to_apply=%region_5.0 | reduce | flops 540672 | bytes 3604484 | tf_op jit(solution)/shard_map/reduce_sum | solution.py:58
  (21 shorter events, 0.2 us)
Async XLA Ops:
  7.2 12.0 %copy-start = (bf16[2048,352]{0,1:T(8,128)(2,1)S(1)}, bf16[2048,352]{0,1:T(8,128)(2,1)}, u32[]{:S(2)}) copy-start(bf16[2048,352]{0,1:T(8,128)(2,1)} %param.9) | copy-start | bytes 4325380
  7.2 79.3 %reduce-scatter.2.cloned.1.call-start = ((), (), s32[]{:S(2)}) async-start(), calls=%async_computation.2 | async-start | bytes 1179648 | tf_op jit(solution)/shard_map/reduce_scatter | solution.py:39
  19.0 1.6 copy-start.4
  19.0 1.6 copy-start.7
  20.6 12.3 %copy-start.2 = (f32[128,352]{0,1:T(8,128)}, f32[128,352]{0,1:T(8,128)S(1)}, u32[]{:S(2)}) copy-start(f32[128,352]{0,1:T(8,128)S(1)} %fusion.3) | copy-start | bytes 540676
  20.6 0.9 copy-start.6
  20.7 11.2 %copy-start.3 = (bf16[352,2048]{1,0:T(8,128)(2,1)S(1)}, bf16[352,2048]{1,0:T(8,128)(2,1)}, u32[]{:S(2)}) copy-start(bf16[352,2048]{1,0:T(8,128)(2,1)} %param.11) | copy-start | bytes 4325380
  21.6 11.4 %copy-start.5 = (f32[128,352]{0,1:T(8,128)}, f32[128,352]{0,1:T(8,128)S(1)}, u32[]{:S(2)}) copy-start(f32[128,352]{0,1:T(8,128)S(1)} %fusion.4) | copy-start | bytes 540676
  31.1 0.8 copy-start.1
  80.5 60.6 %all-to-all-start = ((bf16[4,2,90112]{2,1,0:T(2,128)(2,1)}), bf16[4,2,90112]{2,1,0:T(2,128)(2,1)S(1)}, u32[]{:S(2)}, u32[]{:S(2)}) async-start(bf16[4,2,90112]{2,1,0:T(2,128)(2,1)} %reshape.41), calls=%async_computation.1 | async-start | bytes 2883584 | tf_op jit(solution)/shard_map/all_to_all | solution.py:55
Sparse Core Ops, SparseCore 0:
  34.6 36.2 reduce-scatter.1
where the time goes:
time: 167 us
  blocking collectives  73 us (44%)
  other arithmetic  42.9 us (26%)
  local copies, waits for them, and re-layouts  25.4 us (15%)
  between operations  14.2 us (9%)
  matrix products  6.35 us (4%)
  starting transfers between devices  4.91 us (3%)
    psum x1, blocking collectives, per_device(): lax.psum(jnp.sum(d_in * own_normed, axis=0), ('rep', 'fs', 'tp'))  51.7 us
    unnamed x1, other arithmetic  34.4 us
    all_gather x1, blocking collectives, per_device(): lax.all_gather(inputs, ('fs', 'tp'), axis=0, tiled=True)  11.8 us
    all_gather x1, blocking collectives, per_device(): lax.all_gather(cotangent, ('fs', 'tp'), axis=0, tiled=True)  9.52 us
    unnamed x19, local copies, waits for them, and re-layouts  9.19 us
    all_to_all x1, local copies, waits for them, and re-layouts, per_device(): lax.all_to_all(part_down[None].astype(jnp.bfloat16), 'rep', split_axis=1,...  7.01 us
    convert_element_type x1, local copies, waits for them, and re-layouts, per_device(): part_down[None].astype(jnp.bfloat16)  5.72 us
    all_to_all x1, starting transfers between devices, per_device(): lax.all_to_all(part_down[None].astype(jnp.bfloat16), 'rep', split_axis=1,...  4.87 us
  transfers between devices with their start and end apart: 2, of which 0 were waited for; matrix products, arithmetic and copies ran while one was open for 30% of the time, Pallas kernels for 0%

commit v1 on v0

--- a/solution.py
+++ b/solution.py
@@ -45,7 +45,9 @@
     offset = lax.axis_index(("fs", "tp")) * own_rows
     own_normed = lax.dynamic_slice_in_dim(normed, offset, own_rows, 0)
     own_inv = lax.dynamic_slice_in_dim(inv, offset, own_rows, 0)
-    gain_grad = lax.psum(jnp.sum(d_in * own_normed, axis=0), ("rep", "fs", "tp"))
+    block = jnp.sum(d_in * own_normed, axis=0)
+    terms = lax.all_gather(block, ("rep", "fs", "tp"), axis=0, tiled=False)
+    gain_grad = terms.sum(axis=0)
     scaled = d_in * norm_gain
     input_grad = (
         own_inv * (scaled - own_normed * jnp.mean(scaled * own_normed, axis=-1, keepdims=True))

time: 167 us -> 173 us (1.036)
  blocking collectives: 73 us -> 78.4 us
    all_gather x0 -> x1, blocking collectives: none -> 57.1 us  [per_device(): terms = lax.all_gather(block, ('rep', 'fs', 'tp'), axis=0, tiled=False)]
    psum x1 -> x0, blocking collectives: 51.7 us -> none  [per_device(): lax.psum(jnp.sum(d_in * own_normed, axis=0), ('rep', 'fs', 'tp'))]
  transfers between devices with their start and end apart: 2 -> 2, of which waited for: 0 -> 0; matrix products, arithmetic and copies ran while one was open for 30% -> 29% of each run, Pallas kernels for 0% -> 0%
where the time goes in v1:
time: 173 us
  blocking collectives  78.4 us (45%)
  other arithmetic  43.5 us (25%)
  local copies, waits for them, and re-layouts  25.5 us (15%)
  between operations  14.2 us (8%)
  matrix products  6.35 us (4%)
  starting transfers between devices  4.91 us (3%)
    all_gather x1, blocking collectives, per_device(): terms = lax.all_gather(block, ('rep', 'fs', 'tp'), axis=0, tiled=False)  57.1 us
    unnamed x1, other arithmetic  34.4 us
    all_gather x1, blocking collectives, per_device(): lax.all_gather(inputs, ('fs', 'tp'), axis=0, tiled=True)  11.8 us
    all_gather x1, blocking collectives, per_device(): lax.all_gather(cotangent, ('fs', 'tp'), axis=0, tiled=True)  9.52 us
    unnamed x19, local copies, waits for them, and re-layouts  9.19 us
    all_to_all x1, local copies, waits for them, and re-layouts, per_device(): lax.all_to_all(part_down[None].astype(jnp.bfloat16), 'rep', split_axis=1,...  7.01 us
    convert_element_type x1, local copies, waits for them, and re-layouts, per_device(): part_down[None].astype(jnp.bfloat16)  5.72 us
    all_to_all x1, starting transfers between devices, per_device(): lax.all_to_all(part_down[None].astype(jnp.bfloat16), 'rep', split_axis=1,...  4.87 us
  transfers between devices with their start and end apart: 2, of which 0 were waited for; matrix products, arithmetic and copies ran while one was open for 29% of the time, Pallas kernels for 0%

profile of v1, /device:TPU:0, one launch (start us, length us, event | category | flops | bytes accessed | tf_op | source)
XLA Modules:
  0.0 172.8 jit_solution(10523270191200942209)
XLA Ops:
  7.2 11.8 %all_gather.12 = bf16[128,2048]{1,0:T(8,128)(2,1)S(1)} all-gather(bf16[16,2048]{1,0:T(8,128)(2,1)} %param.6), channel_id=1, replica_groups=mesh['rep'=4,'fs'=4,'tp'=2] {'fs','tp'}, dimensions={0}, use_global_device_ids=true | all-gather | bytes 589824 | tf_op jit(solution)/shard_map/all_gather | solution.py:23
  19.2 1.4 fusion.3
  20.7 0.6 fusion.4
  21.3 0.3 copy-done.6
  21.6 9.5 %all_gather.13 = bf16[128,2048]{1,0:T(8,128)(2,1)S(1)} all-gather(bf16[16,2048]{1,0:T(8,128)(2,1)S(1)} %copy-done.6), channel_id=1, replica_groups=mesh['rep'=4,'fs'=4,'tp'=2] {'fs','tp'}, dimensions={0}, use_global_device_ids=true | all-gather | bytes 589824 | tf_op jit(solution)/shard_map/all_gather | solution.py:24
  31.1 0.8 copy-done.1
  31.9 0.5 convolution_multiply_fusion.1
  32.4 0.5 fusion.6
  33.0 1.5 convolution_add_fusion
  34.5 1.8 %fusion.1 = bf16[1,2048,352]{1,2,0:T(8,128)(2,1)S(1)} fusion(bf16[128,2048]{1,0:T(8,128)(2,1)} %copy-done.1, f32[128,352]{0,1:T(8,128)} %copy-done.5, f32[128,352]{0,1:T(8,128)} %copy-done.2), kind=kOutput, calls=%fused_computation.2 | convolution fusion | flops 186261504 | bytes 2326528 | tf_op jit(solution)/shard_map/dot_general | solution.py:10
  36.3 5.7 %copy.14 = bf16[1,2048,352]{2,0,1:T(2,128)(2,1)} copy(bf16[1,2048,352]{1,2,0:T(8,128)(2,1)S(1)} %fusion.1) | data formatting | bytes 2883584 | tf_op jit(solution)/shard_map/convert_element_type | solution.py:58
  42.0 0.5 broadcast.53
  42.5 34.4 %reduce = bf16[2048,352]{1,0:T(8,128)(2,1)S(1)} reduce(bf16[2048,1,352]{2,1,0:T(2,128)(2,1)} %bitcast.16, bf16[]{:T(256)} %broadcast.53), dimensions={1}, to_apply=%bitcast.7.reduce_sub_computation | reduce | bytes 2883586
  76.9 3.6 %reshape.42 = bf16[4,2,90112]{2,1,0:T(2,128)(2,1)} reshape(bf16[2048,352]{1,0:T(8,128)(2,1)S(1)} %reduce) | data formatting | bytes 2883584
  80.5 4.9 %all-to-all-start = ((bf16[4,2,90112]{2,1,0:T(2,128)(2,1)}), bf16[4,2,90112]{2,1,0:T(2,128)(2,1)S(1)}, u32[]{:S(2)}, u32[]{:S(2)}) async-start(bf16[4,2,90112]{2,1,0:T(2,128)(2,1)} %reshape.42), calls=%async_computation.1 | async-start | bytes 2883584 | tf_op jit(solution)/shard_map/all_to_all | solution.py:57
  85.4 1.1 convert_multiply_fusion
  86.5 1.1 multiply_reduce_fusion
  87.6 57.1 %all-gather = f32[65536]{0:T(1024)S(1)} all-gather(f32[2048]{0:T(1024)S(1)} %get-tuple-element.3), channel_id=2, replica_groups=mesh['rep'=4,'fs'=4,'tp'=2] {'rep','fs','tp'}, dimensions={0}, use_global_device_ids=true | all-gather | bytes 270336 | tf_op jit(solution)/shard_map/all_gather | solution.py:49
  144.8 0.6 reduce_sum.48
  145.4 1.7 multiply_convert_fusion.6
  147.1 4.0 %reshape.43 = bf16[2048,1,352]{2,1,0:T(2,128)(2,1)} reshape(bf16[4,2,90112]{2,1,0:T(2,128)(2,1)S(1)} %all-to-all-done) | data formatting | bytes 2883584
  151.1 7.0 %copy.15 = bf16[1,2048,352]{1,2,0:T(8,128)(2,1)S(1)} copy(bf16[1,2048,352]{2,0,1:T(2,128)(2,1)} %bitcast.17) | data formatting | bytes 2883584 | tf_op jit(solution)/shard_map/all_to_all | solution.py:57
  158.1 3.4 %reshape.40 = f32[4,512,352]{1,0,2:T(4,128)} reshape(bf16[1,2048,352]{1,2,0:T(8,128)(2,1)S(1)} %copy.15) | data formatting | bytes 4325376 | tf_op jit(solution)/shard_map/convert_element_type | solution.py:59
  161.5 4.4 %reduce_sum.49 = f32[512,352]{0,1:T(8,128)} reduce(f32[4,512,352]{1,0,2:T(4,128)} %reshape.40, f32[]{:T(128)} %constant.11.clone.1), dimensions={0}, to_apply=%region_5.0 | reduce | flops 540672 | bytes 3604484 | tf_op jit(solution)/shard_map/reduce_sum | solution.py:60
  (23 shorter events, 0.4 us)
Async XLA Ops:
  7.2 12.0 %copy-start = (bf16[2048,352]{0,1:T(8,128)(2,1)S(1)}, bf16[2048,352]{0,1:T(8,128)(2,1)}, u32[]{:S(2)}) copy-start(bf16[2048,352]{0,1:T(8,128)(2,1)} %param.9) | copy-start | bytes 4325380
  7.2 79.3 %reduce-scatter.2.cloned.1.call-start = ((), (), s32[]{:S(2)}) async-start(), calls=%async_computation.2 | async-start | bytes 1179648 | tf_op jit(solution)/shard_map/reduce_scatter | solution.py:39
  19.0 1.6 copy-start.4
  19.0 1.6 copy-start.7
  20.6 12.3 %copy-start.2 = (f32[128,352]{0,1:T(8,128)}, f32[128,352]{0,1:T(8,128)S(1)}, u32[]{:S(2)}) copy-start(f32[128,352]{0,1:T(8,128)S(1)} %fusion.3) | copy-start | bytes 540676
  20.6 0.9 copy-start.6
  20.7 11.2 %copy-start.3 = (bf16[352,2048]{1,0:T(8,128)(2,1)S(1)}, bf16[352,2048]{1,0:T(8,128)(2,1)}, u32[]{:S(2)}) copy-start(bf16[352,2048]{1,0:T(8,128)(2,1)} %param.11) | copy-start | bytes 4325380
  21.6 11.4 %copy-start.5 = (f32[128,352]{0,1:T(8,128)}, f32[128,352]{0,1:T(8,128)S(1)}, u32[]{:S(2)}) copy-start(f32[128,352]{0,1:T(8,128)S(1)} %fusion.4) | copy-start | bytes 540676
  31.1 0.8 copy-start.1
  80.5 66.6 %all-to-all-start = ((bf16[4,2,90112]{2,1,0:T(2,128)(2,1)}), bf16[4,2,90112]{2,1,0:T(2,128)(2,1)S(1)}, u32[]{:S(2)}, u32[]{:S(2)}) async-start(bf16[4,2,90112]{2,1,0:T(2,128)(2,1)} %reshape.42), calls=%async_computation.1 | async-start | bytes 2883584 | tf_op jit(solution)/shard_map/all_to_all | solution.py:57
Sparse Core Ops, SparseCore 0:
  34.6 36.2 reduce-scatter.1
